TPU v7x, 32 devices: a whole 2x2x4 slice. The times are simulated.
32 devices in a mesh: sp: 16 (over z, y, x), tp: 2 (over core).
Axes of the slice: x: 2, y: 2, z: 4, core: 2. Of those that a mesh axis runs over, the one named last changes fastest.
Arguments:
- tokens: bfloat16 [8192, 2048], P(('sp', 'tp')), may hold values from -6 to 6
- norm_gain: float32 [2048], replicated, may hold values from 0.1 to 1.9
- in_weight: bfloat16 [2048, 1024], P(None, 'tp'), may hold values from -0.125 to 0.125
- gate_weight: bfloat16 [2048, 1024], P(None, 'tp'), may hold values from -0.125 to 0.125
- conv_weight: float32 [4, 1024], P(None, 'tp'), may hold values from -3 to 3
- decay_gate_weight: bfloat16 [16, 64, 64], P('tp'), may hold values from -0.75 to 0.75
- decay_gate_bias: float32 [1024], P('tp'), may hold values from -4 to 4
- input_gate_weight: bfloat16 [16, 64, 64], P('tp'), may hold values from -0.75 to 0.75
- input_gate_bias: float32 [1024], P('tp'), may hold values from -4 to 4
- channel_decay_rate: float32 [1024], P('tp'), may hold values from 4.8828125e-06 to 0.01
- forgetting_offset: float32 [16, 8192], P('tp', 'sp'), may hold values from -1.6 to 0
- out_weight: bfloat16 [1024, 2048], P('tp'), may hold values from -0.1875 to 0.1875
Outputs:
- mixed: bfloat16 [8192, 2048], P(('sp', 'tp'))
All inputs are finite; a program needn't handle non-finite values.
Results may differ from a plain program's by a relative error of at most 0.0067.
Values may be sent and summed in bfloat16 or wider, within the bound.
A program may use at most 64 MiB of HBM per device.

v0:
```python
import jax
import jax.numpy as jnp
from jax import lax
from jax.sharding import PartitionSpec as P

epsilon = 1e-05


def from_behind(value, axis, steps):
    count = lax.axis_size(axis)
    first, last = (max(0, -steps), min(count, count - steps))
    return lax.ppermute(value, axis, [(source, source + steps) for source in range(first, last)])


def prefix(part, axis, combine, identity):
    place = lax.axis_index(axis)
    gathered = jax.tree.map(lambda a: lax.all_gather(a, axis), part)
    state = jax.tree.map(lambda a, e: jnp.zeros_like(a) + jnp.asarray(e, a.dtype), part, identity)

    def one(hop, state):
        return combine(
            state, jax.tree.map(lambda a: lax.dynamic_index_in_dim(a, hop, 0, False), gathered)
        )

    return lax.fori_loop(0, place, one, state)


def link(earlier, later):
    return (earlier[0] * later[0], later[0] * earlier[1] + later[1])


def body(
    tokens,
    norm_gain,
    in_weight,
    gate_weight,
    conv_weight,
    decay_gate_weight,
    decay_gate_bias,
    input_gate_weight,
    input_gate_bias,
    channel_decay_rate,
    forgetting_offset,
    out_weight,
):
    floats = tokens.astype(jnp.float32)
    middle_point = floats - jnp.mean(floats, axis=1, keepdims=True)
    spread = jnp.mean(middle_point * middle_point, axis=1, keepdims=True)
    normed = (middle_point * lax.rsqrt(spread + epsilon) * norm_gain).astype(jnp.bfloat16)
    joined = jnp.concatenate([in_weight, gate_weight], axis=1)
    width = in_weight.shape[1]
    projected = jnp.dot(
        lax.all_gather(normed, "tp", axis=0, tiled=True), joined, preferred_element_type=jnp.float32
    ).astype(jnp.bfloat16)
    inner = projected[:, :width]
    gate = projected[:, width:]
    length = inner.shape[0]
    taps = conv_weight.shape[0]
    before = from_behind(inner[length - taps + 1 :], "sp", 1)
    extended = jnp.concatenate([before, inner], axis=0)
    smooth = extended[0:length].astype(jnp.float32) * conv_weight[0]
    for tap in range(1, taps):
        smooth = smooth + extended[tap : tap + length].astype(jnp.float32) * conv_weight[tap]
    smoothed = smooth.astype(jnp.bfloat16)
    heads = decay_gate_weight.shape[0]
    block = decay_gate_weight.shape[1]
    grouped = smoothed.reshape(length, heads, block)
    retain = jax.nn.sigmoid(
        jnp.einsum(
            "rhi,hij->rhj", grouped, decay_gate_weight, preferred_element_type=jnp.float32
        ).reshape(length, width)
        + decay_gate_bias
    )
    admit = jax.nn.sigmoid(
        jnp.einsum(
            "rhi,hij->rhj", grouped, input_gate_weight, preferred_element_type=jnp.float32
        ).reshape(length, width)
        + input_gate_bias
    )
    log_decay = -8.0 * retain * channel_decay_rate + jnp.repeat(forgetting_offset.T, block, axis=1)
    decay = jnp.exp(log_decay)
    drive = jnp.sqrt(-jnp.expm1(2.0 * log_decay)) * admit * smoothed.astype(jnp.float32)
    local = lax.associative_scan(link, (decay, drive), axis=0)
    carried = prefix(
        (local[0][length - 1], local[1][length - 1]),
        "sp",
        link,
        (jnp.ones((width,), jnp.float32), jnp.zeros((width,), jnp.float32)),
    )
    state = local[1] + local[0] * carried[1]
    gated = (state * jax.nn.gelu(gate.astype(jnp.float32))).astype(jnp.bfloat16)
    by_token = lax.all_to_all(gated, "tp", split_axis=0, concat_axis=1, tiled=True)
    full_rows = lax.all_gather(out_weight, "tp", axis=0, tiled=True)
    result = jnp.dot(by_token, full_rows, preferred_element_type=jnp.float32)
    return result.astype(jnp.bfloat16)


def solution(mesh):
    placed = (
        P(("sp", "tp"), None),
        P(),
        P(None, "tp"),
        P(None, "tp"),
        P(None, "tp"),
        P("tp", None, None),
        P("tp"),
        P("tp", None, None),
        P("tp"),
        P("tp"),
        P("tp", "sp"),
        P("tp", None),
    )
    return jax.shard_map(
        body, mesh=mesh, in_specs=placed, out_specs=P(("sp", "tp"), None), check_vma=False
    )
```

profile of v0, /device:TPU:0, one launch (start us, length us, event | category | flops | bytes accessed | tf_op | source)
XLA Modules:
  0.0 247.2 jit_solution(12234796272308864339)
XLA Ops:
  6.5 1.5 convert_reduce_fusion
  8.1 1.6 fusion.6
  9.8 1.4 fusion.8
  12.0 12.6 %all-gather.5.cloned.1.call-done = bf16[512,2048]{1,0:T(8,128)(2,1)} async-done(((bf16[256,2048]{1,0:T(8,128)(2,1)}), bf16[512,2048]{1,0:T(8,128)(2,1)}) %all-gather.5.cloned.1.call-update) | async-done | bytes 2097168 | tf_op jit(solution)/shard_map/all_gather | solution.py:53
  24.6 5.2 %fusion.9 = bf16[512,1024]{1,0:T(8,128)(2,1)S(1)} fusion(bf16[512,2048]{1,0:T(8,128)(2,1)} %all-gather.5.cloned.1.call-done, bf16[2048,512]{1,0:T(8,128)(2,1)} %param.17, bf16[2048,512]{1,0:T(8,128)(2,1)} %param.16), kind=kOutput, calls=%fused_computation.19 | convolution fusion | flops 2156396544 | bytes 7340032 | tf_op jit(solution)/shard_map/dot_general | solution.py:52
  29.8 3.6 %collective-permute-start = (bf16[3,512]{1,0:T(4,128)(2,1)S(1)}, bf16[3,512]{1,0:T(4,128)(2,1)S(1)}, u32[]{:S(2)}, u32[]{:S(2)}) collective-permute-start(bf16[3,512]{1,0:T(4,128)(2,1)S(1)} %slice.393), channel_id=1, source_target_pairs={{0,2},{2,4},{4,6},{6,8},{8,10},{10,12},{12,14},{14,16},{16,18},{18... | collective-permute-start | bytes 9224 | tf_op jit(solution)/shard_map/ppermute | solution.py:12
  33.6 1.3 copy.30
  36.1 1.3 copy.29
  39.1 3.0 %convert_multiply_fusion.3 = (f32[512,512]{1,0:T(8,128)S(1)}, f32[512,512]{1,0:T(8,128)S(1)}) fusion(bf16[512,512]{1,0:T(8,128)(2,1)S(1)} %add_convert_fusion, f32[512,512]{1,0:T(8,128)} %copy.32, f32[512]{0:T(512)S(1)} %copy-done.38, f32[512,512]{1,0:T(8,128)} %copy.30, f32[512]{0:T(512)S(1)} %broadcast_multiply_fusion, f32[512,512]{1,0:T(8,128)} %copy.29, ...), kind=kLoop, calls=%fused_computation.27 | loop fusion | flops 3932160 | bytes 5773312 | tf_op jit(solution)/shard_map/mul | solution.py:82
  42.1 2.1 slice.309
  44.2 2.1 slice.310
  46.3 2.1 slice.308
  48.4 2.1 slice.312
  50.4 1.7 multiply_add_fusion.2
  52.2 1.4 slice.315
  53.5 1.4 slice.316
  54.9 1.4 slice.314
  56.3 1.4 slice.318
  57.6 2.0 multiply_add_fusion.3
  61.0 1.6 slice.320
  62.6 1.6 slice.324
  64.2 1.8 multiply_add_fusion.4
  66.0 1.5 slice.327
  67.6 1.5 slice.328
  69.1 1.5 slice.326
  70.6 1.5 slice.330
  72.2 1.6 multiply_add_fusion.5
  73.8 1.4 slice.333
  75.2 1.4 slice.334
  76.6 1.5 slice.332
  78.1 1.4 slice.336
  79.5 1.4 multiply_add_fusion.6
  81.0 1.4 slice.339
  82.3 1.4 slice.340
  83.7 1.4 slice.338
  85.1 1.4 slice.342
  86.4 1.4 multiply_add_fusion.7
  89.0 1.3 slice.344
  90.3 1.3 slice.348
  91.6 1.4 multiply_add_fusion.8
  98.9 1.4 fusion.34
  100.9 1.3 slice.343
  102.9 1.3 slice.434
  105.5 1.4 slice.362
  109.5 1.4 slice.331
  110.9 1.4 slice.364
  113.7 1.3 slice.403
  115.0 1.5 slice.325
  116.5 1.5 slice.366
  118.1 1.3 slice.431
  120.7 1.6 slice.319
  125.1 1.4 slice.313
  126.5 1.4 slice.370
  129.0 2.1 slice.307
  131.1 2.1 slice.372
  138.8 2.3 fusion.21
  141.4 41.5 %all-gather.1 = f32[16,1,512]{2,1,0:T(1,128)S(1)} all-gather(f32[1,1,512]{2,1,0:T(1,128)S(1)} %add_bitcast_fusion), channel_id=1, replica_groups=mesh['sp'=16,'tp'=2] {'sp'}, dimensions={0}, use_global_device_ids=true | all-gather | bytes 34816 | tf_op jit(solution)/shard_map/all_gather | solution.py:17
  182.9 2.1 pad.145
  185.0 1.9 pad_maximum_fusion.2
  186.9 4.6 %pad.144 = f32[512,512]{1,0:T(8,128)} pad(f32[256,512]{1,0:T(8,128)} %pad_maximum_fusion.2, f32[]{:T(128)} %constant.15.clone.1), padding=0_1_1x0_0_0 | pad | bytes 1572868 | tf_op jit(solution)/shard_map/pad | solution.py:83
  192.2 35.6 %all-gather = f32[16,1,512]{2,1,0:T(1,128)S(1)} all-gather(f32[1,1,512]{2,1,0:T(1,128)S(1)} %add_bitcast_fusion.1), channel_id=1, replica_groups=mesh['sp'=16,'tp'=2] {'sp'}, dimensions={0}, use_global_device_ids=true | all-gather | bytes 34816 | tf_op jit(solution)/shard_map/all_gather | solution.py:17
  227.8 2.7 %fusion.18 = bf16[512,512]{1,0:T(8,128)(2,1)} fusion(f32[512,512]{1,0:T(8,128)} %pad.144, f32[512,512]{1,0:T(8,128)S(1)} %pad.145, f32[512,512]{1,0:T(8,128)S(1)} %pad.126, f32[512,512]{1,0:T(8,128)S(1)} %pad.127, bf16[512,1024]{1,0:T(8,128)(2,1)} %copy-done.2, f32[512]{0:T(512)S(1)} %get-tuple-element.49), kind=kLoop, calls=%fused_computation.26 | loop fusion | flops 3932160 | bytes 5244928 | tf_op jit(solution)/shard_map/convert_element_type | solution.py:91
  231.8 4.2 %all_to_all.19 = bf16[2,256,512]{1,2,0:T(8,128)(2,1)S(1)} all-to-all(bf16[2,256,512]{1,2,0:T(8,128)(2,1)S(1)} %copy.33), channel_id=1, replica_groups=mesh['sp'=16,'tp'=2] {'tp'}, dimensions={0} | all-to-all | bytes 1048576 | tf_op jit(solution)/shard_map/all_to_all | solution.py:92
  236.0 4.4 %convolution_convert_fusion = bf16[256,2048]{1,0:T(8,128)(2,1)} fusion(bf16[256,1024]{0,1:T(8,128)(2,1)S(1)} %bitcast.46, bf16[1024,2048]{1,0:T(8,128)(2,1)} %all-gather.7.cloned.1.call-done), kind=kOutput, calls=%fused_computation.9 | convolution fusion | flops 1074266112 | bytes 5767168 | tf_op jit(solution)/shard_map/dot_general | solution.py:94
  (196 shorter events, 31.0 us)
Async XLA Ops:
  6.5 29.2 %copy-start = (bf16[8,64,64]{2,1,0:T(8,128)(2,1)S(1)}, bf16[8,64,64]{2,1,0:T(8,128)(2,1)}, u32[]{:S(2)}) copy-start(bf16[8,64,64]{2,1,0:T(8,128)(2,1)} %param.19) | copy-start | bytes 196612
  6.5 3.2 %copy-start.1 = (bf16[256,2048]{1,0:T(8,128)(2,1)S(1)}, bf16[256,2048]{1,0:T(8,128)(2,1)}, u32[]{:S(2)}) copy-start(bf16[256,2048]{1,0:T(8,128)(2,1)} %param.14) | copy-start | bytes 3145732
  6.5 3.2 %copy-start.18 = (f32[2048]{0:T(1024)S(1)}, f32[2048]{0:T(1024)}, u32[]{:S(2)}) copy-start(f32[2048]{0:T(1024)} %param.15) | copy-start | bytes 24580
  6.5 18.1 %all-gather.5.cloned.1.call-start = ((), (), s32[]{:S(2)}) async-start(), calls=%async_computation.1 | async-start | bytes 3145728 | tf_op jit(solution)/shard_map/all_gather | solution.py:53
  11.1 0.8 copy-start.33
  11.2 224.8 %all-gather.7.cloned.1.call-start = ((), (), s32[]{:S(2)}) async-start(), calls=%async_computation.2 | async-start | bytes 6291456 | tf_op jit(solution)/shard_map/all_gather | solution.py:93
  11.9 21.5 %copy-start.40 = (f32[512]{0:T(512)S(1)}, f32[512]{0:T(512)}, u32[]{:S(2)}) copy-start(f32[512]{0:T(512)} %param.23) | copy-start | bytes 6148
  11.9 21.5 %copy-start.15 = (f32[8,512]{1,0:T(8,128)S(1)}, f32[8,512]{1,0:T(8,128)}, u32[]{:S(2)}) copy-start(f32[8,512]{1,0:T(8,128)} %param.24) | copy-start | bytes 49156
  29.8 5.2 %copy-start.2 = (bf16[512,1024]{1,0:T(8,128)(2,1)}, bf16[512,1024]{1,0:T(8,128)(2,1)S(1)}, u32[]{:S(2)}) copy-start(bf16[512,1024]{1,0:T(8,128)(2,1)S(1)} %fusion.9) | copy-start | bytes 3145732
  29.8 5.2 %collective-permute-start = (bf16[3,512]{1,0:T(4,128)(2,1)S(1)}, bf16[3,512]{1,0:T(4,128)(2,1)S(1)}, u32[]{:S(2)}, u32[]{:S(2)}) collective-permute-start(bf16[3,512]{1,0:T(4,128)(2,1)S(1)} %slice.393), channel_id=1, source_target_pairs={{0,2},{2,4},{4,6},{6,8},{8,10},{10,12},{12,14},{14,16},{16,18},{18... | collective-permute-start | bytes 9224 | tf_op jit(solution)/shard_map/ppermute | solution.py:12
  35.7 1.7 copy-start.11
  37.4 1.7 copy-start.38
  37.4 1.7 copy-start.39
  124.9 9.5 %copy-start.34 = (f32[1,512]{1,0:T(1,128)S(1)}, f32[1,512]{1,0:T(1,128)}, u32[]{:S(2)}) copy-start(f32[1,512]{1,0:T(1,128)} %get-tuple-element.90) | copy-start | bytes 6148
  124.9 9.5 %copy-start.35 = (f32[1,512]{1,0:T(1,128)S(1)}, f32[1,512]{1,0:T(1,128)}, u32[]{:S(2)}) copy-start(f32[1,512]{1,0:T(1,128)} %get-tuple-element.91) | copy-start | bytes 6148
  125.0 9.5 %copy-start.36 = (f32[1,512]{1,0:T(1,128)S(1)}, f32[1,512]{1,0:T(1,128)}, u32[]{:S(2)}) copy-start(f32[1,512]{1,0:T(1,128)} %get-tuple-element.92) | copy-start | bytes 6148
  125.0 9.5 %copy-start.37 = (f32[1,512]{1,0:T(1,128)S(1)}, f32[1,512]{1,0:T(1,128)}, u32[]{:S(2)}) copy-start(f32[1,512]{1,0:T(1,128)} %get-tuple-element.93) | copy-start | bytes 6148
  125.0 9.5 %copy-start.17 = (f32[2,512]{1,0:T(2,128)S(1)}, f32[2,512]{1,0:T(2,128)}, u32[]{:S(2)}) copy-start(f32[2,512]{1,0:T(2,128)} %get-tuple-element.107) | copy-start | bytes 12292
  125.0 9.5 %copy-start.16 = (f32[2,512]{1,0:T(2,128)S(1)}, f32[2,512]{1,0:T(2,128)}, u32[]{:S(2)}) copy-start(f32[2,512]{1,0:T(2,128)} %get-tuple-element.106) | copy-start | bytes 12292
  125.0 9.6 %copy-start.13 = (f32[3,512]{1,0:T(4,128)S(1)}, f32[3,512]{1,0:T(4,128)}, u32[]{:S(2)}) copy-start(f32[3,512]{1,0:T(4,128)} %slice.343) | copy-start | bytes 18436
  125.0 9.6 %copy-start.14 = (f32[3,512]{1,0:T(4,128)S(1)}, f32[3,512]{1,0:T(4,128)}, u32[]{:S(2)}) copy-start(f32[3,512]{1,0:T(4,128)} %slice.360) | copy-start | bytes 18436
  125.0 9.6 %copy-start.32 = (f32[1,512]{1,0:T(1,128)S(1)}, f32[1,512]{1,0:T(1,128)}, u32[]{:S(2)}) copy-start(f32[1,512]{1,0:T(1,128)} %slice.434) | copy-start | bytes 6148
  125.0 9.7 %copy-start.31 = (f32[1,512]{1,0:T(1,128)S(1)}, f32[1,512]{1,0:T(1,128)}, u32[]{:S(2)}) copy-start(f32[1,512]{1,0:T(1,128)} %slice.405) | copy-start | bytes 6148
  125.0 9.7 %copy-start.12 = (f32[7,512]{1,0:T(8,128)S(1)}, f32[7,512]{1,0:T(8,128)}, u32[]{:S(2)}) copy-start(f32[7,512]{1,0:T(8,128)} %slice.362) | copy-start | bytes 43012
  125.0 9.8 %copy-start.30 = (f32[1,512]{1,0:T(1,128)S(1)}, f32[1,512]{1,0:T(1,128)}, u32[]{:S(2)}) copy-start(f32[1,512]{1,0:T(1,128)} %slice.433) | copy-start | bytes 6148
  125.0 9.8 %copy-start.29 = (f32[1,512]{1,0:T(1,128)S(1)}, f32[1,512]{1,0:T(1,128)}, u32[]{:S(2)}) copy-start(f32[1,512]{1,0:T(1,128)} %slice.404) | copy-start | bytes 6148
  125.0 9.9 %copy-start.9 = (f32[15,512]{1,0:T(8,128)S(1)}, f32[15,512]{1,0:T(8,128)}, u32[]{:S(2)}) copy-start(f32[15,512]{1,0:T(8,128)} %slice.331) | copy-start | bytes 92164
  125.1 9.9 %copy-start.10 = (f32[15,512]{1,0:T(8,128)S(1)}, f32[15,512]{1,0:T(8,128)}, u32[]{:S(2)}) copy-start(f32[15,512]{1,0:T(8,128)} %slice.364) | copy-start | bytes 92164
  126.5 8.5 %copy-start.28 = (f32[1,512]{1,0:T(1,128)S(1)}, f32[1,512]{1,0:T(1,128)}, u32[]{:S(2)}) copy-start(f32[1,512]{1,0:T(1,128)} %slice.432) | copy-start | bytes 6148
  126.5 8.6 %copy-start.27 = (f32[1,512]{1,0:T(1,128)S(1)}, f32[1,512]{1,0:T(1,128)}, u32[]{:S(2)}) copy-start(f32[1,512]{1,0:T(1,128)} %slice.403) | copy-start | bytes 6148
  129.0 6.1 %copy-start.7 = (f32[31,512]{1,0:T(8,128)S(1)}, f32[31,512]{1,0:T(8,128)}, u32[]{:S(2)}) copy-start(f32[31,512]{1,0:T(8,128)} %slice.325) | copy-start | bytes 190468
  129.0 6.1 %copy-start.8 = (f32[31,512]{1,0:T(8,128)S(1)}, f32[31,512]{1,0:T(8,128)}, u32[]{:S(2)}) copy-start(f32[31,512]{1,0:T(8,128)} %slice.366) | copy-start | bytes 190468
  131.1 4.1 %copy-start.26 = (f32[1,512]{1,0:T(1,128)S(1)}, f32[1,512]{1,0:T(1,128)}, u32[]{:S(2)}) copy-start(f32[1,512]{1,0:T(1,128)} %slice.431) | copy-start | bytes 6148
  131.1 4.2 %copy-start.25 = (f32[1,512]{1,0:T(1,128)S(1)}, f32[1,512]{1,0:T(1,128)}, u32[]{:S(2)}) copy-start(f32[1,512]{1,0:T(1,128)} %slice.402) | copy-start | bytes 6148
  134.7 0.9 copy-start.5
  134.7 1.0 copy-start.6
  135.0 0.8 copy-start.24
  135.2 0.7 copy-start.23
  135.8 1.0 copy-start.3
  135.8 1.0 copy-start.4
  136.0 1.0 copy-start.22
  137.1 0.7 copy-start.21
  138.8 2.3 copy-start.20
  141.2 43.8 %copy-start.19 = (f32[1,512]{1,0:T(1,128)S(1)}, f32[1,512]{1,0:T(1,128)}, u32[]{:S(2)}) copy-start(f32[1,512]{1,0:T(1,128)} %slice.428) | copy-start | bytes 6148
Sparse Core Ops, SparseCore 0:
  11.3 13.2 all-gather.4
  26.1 14.8 all-gather.6
where the time goes:
time: 250 us; the launch traced here: 247 us
  local copies, waits for them, and re-layouts  92.7 us (37%)
  blocking collectives  81.3 us (33%)
  other arithmetic  31.5 us (13%)
  between operations  14.4 us (6%)
  waiting for transfers between devices  13.4 us (5%)
  matrix products  10.3 us (4%)
  starting transfers between devices  3.68 us (1%)
    slice x60, local copies, waits for them, and re-layouts, body(): local = lax.associative_scan(link, (decay, drive), axis=0)  78 us
    all_gather x2, blocking collectives, prefix(): gathered = jax.tree.map(lambda a: lax.all_gather(a, axis), part)  77.1 us
    add x16, other arithmetic, link(): return (earlier[0] * later[0], later[0] * earlier[1] + later[1])  14.7 us
    all_gather x1, waiting for transfers between devices, body(): lax.all_gather(normed, 'tp', axis=0, tiled=True)  12.6 us
    pad x32, local copies, waits for them, and re-layouts, body(): local = lax.associative_scan(link, (decay, drive), axis=0)  7.67 us
    dot_general x1, matrix products, body(): jnp.dot(lax.all_gather(normed, 'tp', axis=0, tiled=True), joined, preferr...  5.18 us
  transfers between devices with their start and end apart: 3, of which 1 were waited for; matrix products, arithmetic and copies ran while one was open for 50% of the time, Pallas kernels for 0%

commit v1 on v0

--- a/solution.py
+++ b/solution.py
@@ -1,6 +1,10 @@
+import functools
+
 import jax
 import jax.numpy as jnp
 from jax import lax
+from jax.experimental import pallas as pl
+from jax.experimental.pallas import tpu as pltpu
 from jax.sharding import PartitionSpec as P
 
 epsilon = 1e-05
@@ -12,21 +16,115 @@
     return lax.ppermute(value, axis, [(source, source + steps) for source in range(first, last)])
 
 
-def prefix(part, axis, combine, identity):
-    place = lax.axis_index(axis)
-    gathered = jax.tree.map(lambda a: lax.all_gather(a, axis), part)
-    state = jax.tree.map(lambda a, e: jnp.zeros_like(a) + jnp.asarray(e, a.dtype), part, identity)
-
-    def one(hop, state):
-        return combine(
-            state, jax.tree.map(lambda a: lax.dynamic_index_in_dim(a, hop, 0, False), gathered)
+LANES = 128
+PIECES = 8
+
+
+def scan_kernel(decay_ref, drive_ref, ends_ref, local_ref, product_ref):
+    steps = decay_ref.shape[0] // PIECES
+
+    def one(j, carry):
+        p, h = carry
+        rows = pl.ds(j, PIECES, stride=steps)
+        a = decay_ref[rows, :]
+        h = a * h + drive_ref[rows, :]
+        p = a * p
+        local_ref[rows, :] = h
+        product_ref[rows, :] = p
+        return p, h
+
+    zero = jnp.zeros((PIECES, LANES), jnp.float32)
+    p, h = lax.fori_loop(0, steps, one, (zero + 1.0, zero), unroll=8)
+    before_h = h[0:1]
+    before_p = p[0:1]
+    for piece in range(1, PIECES):
+        rows = pl.ds(piece * steps, steps)
+        part = product_ref[rows, :]
+        local_ref[rows, :] = local_ref[rows, :] + part * before_h
+        product_ref[rows, :] = part * before_p
+        before_h = p[piece : piece + 1] * before_h + h[piece : piece + 1]
+        before_p = p[piece : piece + 1] * before_p
+    ends_ref[0:1, :] = before_p
+    ends_ref[1:2, :] = before_h
+
+
+def local_scan(decay, drive):
+    length, width = decay.shape
+    block = pl.BlockSpec((length, LANES), lambda i: (0, i))
+    whole = jax.ShapeDtypeStruct((length, width), jnp.float32)
+    return pl.pallas_call(
+        scan_kernel,
+        grid=(width // LANES,),
+        in_specs=[block, block],
+        out_specs=[pl.BlockSpec((2, LANES), lambda i: (0, i)), block, block],
+        out_shape=[jax.ShapeDtypeStruct((2, width), jnp.float32), whole, whole],
+        name="local_scan",
+    )(decay, drive)
+
+
+def prefix_kernel(count, ends_ref, carry_ref, slots, send_sem, recv_sem):
+    me = lax.axis_index("sp")
+    barrier = pltpu.get_barrier_semaphore()
+
+    def greet(k, _):
+        pl.semaphore_signal(
+            barrier,
+            inc=1,
+            device_id={"sp": lax.rem(me + k, count)},
+            device_id_type=pl.DeviceIdType.MESH,
         )
-
-    return lax.fori_loop(0, place, one, state)
-
-
-def link(earlier, later):
-    return (earlier[0] * later[0], later[0] * earlier[1] + later[1])
+        return 0
+
+    lax.fori_loop(1, count, greet, 0)
+    pl.semaphore_wait(barrier, count - 1)
+
+    def copy(source, target):
+        return pltpu.make_async_remote_copy(
+            src_ref=ends_ref,
+            dst_ref=slots.at[source],
+            send_sem=send_sem.at[target],
+            recv_sem=recv_sem.at[source],
+            device_id={"sp": target},
+            device_id_type=pl.DeviceIdType.MESH,
+        )
+
+    def send(target, _):
+        copy(me, target).start()
+        return 0
+
+    lax.fori_loop(me + 1, count, send, 0)
+    carry_ref[...] = jnp.zeros_like(carry_ref)
+
+    def receive(source, _):
+        copy(source, me).wait_recv()
+        carry_ref[...] = slots[source, 0:1, :] * carry_ref[...] + slots[source, 1:2, :]
+        return 0
+
+    lax.fori_loop(0, me, receive, 0)
+
+    def sent(target, _):
+        copy(me, target).wait_send()
+        return 0
+
+    lax.fori_loop(me + 1, count, sent, 0)
+
+
+def prefix(ends):
+    count = lax.axis_size("sp")
+    width = ends.shape[1]
+    return pl.pallas_call(
+        functools.partial(prefix_kernel, count),
+        in_specs=[pl.BlockSpec(memory_space=pltpu.VMEM)],
+        out_specs=pl.BlockSpec(memory_space=pltpu.VMEM),
+        out_shape=jax.ShapeDtypeStruct((1, width), jnp.float32),
+        scratch_shapes=[
+            pltpu.VMEM((count, 2, width), jnp.float32),
+            pltpu.SemaphoreType.DMA((count,)),
+            pltpu.SemaphoreType.DMA((count,)),
+        ],
+        compiler_params=pltpu.CompilerParams(collective_id=0, has_side_effects=True),
+        name="prefix",
+    )(ends)
 
 
 def body(
@@ -80,14 +178,8 @@
     log_decay = -8.0 * retain * channel_decay_rate + jnp.repeat(forgetting_offset.T, block, axis=1)
     decay = jnp.exp(log_decay)
     drive = jnp.sqrt(-jnp.expm1(2.0 * log_decay)) * admit * smoothed.astype(jnp.float32)
-    local = lax.associative_scan(link, (decay, drive), axis=0)
-    carried = prefix(
-        (local[0][length - 1], local[1][length - 1]),
-        "sp",
-        link,
-        (jnp.ones((width,), jnp.float32), jnp.zeros((width,), jnp.float32)),
-    )
-    state = local[1] + local[0] * carried[1]
+    ends, local, product = local_scan(decay, drive)
+    state = local + product * prefix(ends)
     gated = (state * jax.nn.gelu(gate.astype(jnp.float32))).astype(jnp.bfloat16)
     by_token = lax.all_to_all(gated, "tp", split_axis=0, concat_axis=1, tiled=True)
     full_rows = lax.all_gather(out_weight, "tp", axis=0, tiled=True)

time: 250 us -> 76.7 us (0.31)
  local copies, waits for them, and re-layouts: 92.7 us -> 3.63 us
  blocking collectives: 81.3 us -> 4.15 us
  other arithmetic: 31.5 us -> 11.1 us
  Pallas kernels: 0 us -> 14.6 us
    slice x60 -> x0, local copies, waits for them, and re-layouts: 78 us -> none  [body(): local = lax.associative_scan(link, (decay, drive), axis=0)]
    all_gather x2 -> x0, blocking collectives: 77.1 us -> none  [prefix(): gathered = jax.tree.map(lambda a: lax.all_gather(a, axis), part)]
    add x31 -> x0, other arithmetic: 16.4 us -> none  [the longest x16 14.7 us: link(): return (earlier[0] * later[0], later[0] * earlier[1] + later[1])]
    pallas_call x0 -> x2, Pallas kernels: none -> 14.6 us  [the longest x1 9.25 us: prefix(): pl.pallas_call(functools.partial(prefix_kernel, count), in_specs=[pl.Bloc...]
    pad x32 -> x0, local copies, waits for them, and re-layouts: 7.67 us -> none  [body(): local = lax.associative_scan(link, (decay, drive), axis=0)]
  transfers between devices with their start and end apart: 3 -> 3, of which waited for: 1 -> 2; matrix products, arithmetic and copies ran while one was open for 50% -> 21% of each run, Pallas kernels for 0% -> 19%
where the time goes in v1:
time: 76.7 us; the launch traced here: 75.2 us
  Pallas kernels  14.6 us (19%)
  waiting for transfers between devices  14.1 us (18%)
  between operations  13.6 us (18%)
  other arithmetic  11.1 us (14%)
  matrix products  10.3 us (13%)
  blocking collectives  4.15 us (5%)
  starting transfers between devices  3.68 us (5%)
  local copies, waits for them, and re-layouts  3.63 us (5%)
    all_gather x1, waiting for transfers between devices, body(): lax.all_gather(normed, 'tp', axis=0, tiled=True)  12.6 us
    pallas_call x1, Pallas kernels, prefix(): pl.pallas_call(functools.partial(prefix_kernel, count), in_specs=[pl.Bloc...  9.25 us
    pallas_call x1, Pallas kernels, local_scan(): pl.pallas_call(scan_kernel, grid=(width // LANES,), in_specs=[block, bloc...  5.39 us
    dot_general x1, matrix products, body(): jnp.dot(lax.all_gather(normed, 'tp', axis=0, tiled=True), joined, preferr...  5.18 us
    dot_general x1, matrix products, body(): result = jnp.dot(by_token, full_rows, preferred_element_type=jnp.float32)  4.43 us
    all_to_all x1, blocking collectives, body(): lax.all_to_all(gated, 'tp', split_axis=0, concat_axis=1, tiled=True)  4.15 us
    mul x1, other arithmetic, body(): jnp.sqrt(-jnp.expm1(2.0 * log_decay)) * admit * smoothed.astype(jnp.float32)  4.03 us
    ppermute x1, starting transfers between devices, from_behind(): lax.ppermute(value, axis, [(source, source + steps) for source in range(f...  3.64 us
  transfers between devices with their start and end apart: 3, of which 2 were waited for; matrix products, arithmetic and copies ran while one was open for 21% of the time, Pallas kernels for 19%

profile of v1, /device:TPU:0, one launch (start us, length us, event | category | flops | bytes accessed | tf_op | source)
XLA Modules:
  0.0 75.2 jit_solution(3519279002210851444)
XLA Ops:
  6.5 0.0 copy-start
  6.5 0.0 copy-start.1
  6.5 0.0 copy-start.6
  6.5 0.0 all-gather.3.cloned.1.call-start
  6.5 1.5 %convert_reduce_fusion = f32[256]{0:T(256)S(1)} fusion(bf16[256,2048]{1,0:T(8,128)(2,1)} %param.12), kind=kLoop, calls=%fused_computation.5 | loop fusion | flops 1048320 | bytes 1049600 | tf_op jit(solution)/shard_map/reduce_sum | solution.py:145
  8.1 1.6 %fusion.6 = f32[256]{0:T(256)S(1)} fusion(bf16[256,2048]{1,0:T(8,128)(2,1)} %param.12, f32[256]{0:T(256)S(1)} %broadcast_multiply_fusion.1), kind=kLoop, calls=%fused_computation.9 | loop fusion | flops 2096896 | bytes 1050624 | tf_op jit(solution)/shard_map/reduce_sum | solution.py:146
  9.8 0.0 copy-done.1
  9.8 0.0 copy-done.6
  9.8 1.4 %fusion.8 = bf16[256,2048]{1,0:T(8,128)(2,1)} fusion(bf16[256,2048]{1,0:T(8,128)(2,1)S(1)} %copy-done.1, f32[2048]{0:T(1024)S(1)} %copy-done.6, f32[256]{0:T(256)S(1)} %add_rsqrt_fusion, f32[256]{0:T(256)S(1)} %broadcast_multiply_fusion.1), kind=kLoop, calls=%fused_computation.11 | loop fusion | flops 2621440 | bytes 2107392 | tf_op jit(solution)/shard_map/convert_element_type | solution.py:147
  11.1 0.0 copy-start.7
  11.1 0.0 all-gather.3.cloned.1.call-update
  11.2 0.0 all-gather.5.cloned.1.call-start
  11.2 0.7 all-gather.5.cloned.1.call-update
  11.9 0.0 copy-done.7
  11.9 0.0 copy-start.10
  11.9 0.0 copy-start.5
  12.0 12.6 %all-gather.3.cloned.1.call-done = bf16[512,2048]{1,0:T(8,128)(2,1)} async-done(((bf16[256,2048]{1,0:T(8,128)(2,1)}), bf16[512,2048]{1,0:T(8,128)(2,1)}) %all-gather.3.cloned.1.call-update) | async-done | bytes 2097168 | tf_op jit(solution)/shard_map/all_gather | solution.py:151
  24.6 5.2 %fusion.9 = bf16[512,1024]{1,0:T(8,128)(2,1)S(1)} fusion(bf16[512,2048]{1,0:T(8,128)(2,1)} %all-gather.3.cloned.1.call-done, bf16[2048,512]{1,0:T(8,128)(2,1)} %param.15, bf16[2048,512]{1,0:T(8,128)(2,1)} %param.14), kind=kOutput, calls=%fused_computation.16 | convolution fusion | flops 2156396544 | bytes 7340032 | tf_op jit(solution)/shard_map/dot_general | solution.py:150
  29.8 0.0 copy-start.2
  29.8 3.6 %collective-permute-start = (bf16[3,512]{1,0:T(4,128)(2,1)S(1)}, bf16[3,512]{1,0:T(4,128)(2,1)S(1)}, u32[]{:S(2)}, u32[]{:S(2)}) collective-permute-start(bf16[3,512]{1,0:T(4,128)(2,1)S(1)} %slice.41), channel_id=1, source_target_pairs={{0,2},{2,4},{4,6},{6,8},{8,10},{10,12},{12,14},{14,16},{16,18},{18... | collective-permute-start | bytes 9224 | tf_op jit(solution)/shard_map/ppermute | solution.py:16
  33.5 0.0 copy-done.10
  33.5 0.0 copy-done.5
  33.5 0.1 broadcast_in_dim.2
  33.6 0.3 copy.23
  34.0 0.0 copy-done.2
  34.0 0.8 %collective-permute-done = bf16[3,512]{1,0:T(4,128)(2,1)S(1)} collective-permute-done((bf16[3,512]{1,0:T(4,128)(2,1)S(1)}, bf16[3,512]{1,0:T(4,128)(2,1)S(1)}, u32[]{:S(2)}, u32[]{:S(2)}) %collective-permute-start) | collective-permute-done | bytes 3104 | tf_op jit(solution)/shard_map/ppermute | solution.py:16
  34.8 0.5 add_convert_fusion
  35.3 0.2 copy.20
  35.5 0.0 copy-start.4
  35.5 0.0 copy-done
  35.5 0.3 fusion.24
  35.9 1.4 %copy.22 = f32[512,512]{1,0:T(8,128)} copy(f32[512,512]{0,1:T(8,128)S(1)} %bitcast.29) | data formatting | bytes 2097152 | tf_op jit(solution)/shard_map/reshape | solution.py:169
  37.2 0.0 copy-done.4
  37.2 0.0 copy-start.8
  37.2 0.0 copy-start.9
  37.2 0.3 fusion.25
  37.6 1.3 %copy.25 = f32[512,512]{1,0:T(8,128)} copy(f32[512,512]{0,1:T(8,128)S(1)} %bitcast.28) | data formatting | bytes 2097152 | tf_op jit(solution)/shard_map/reshape | solution.py:175
  38.9 0.0 copy-done.8
  38.9 0.0 copy-done.9
  38.9 4.0 %convert_multiply_fusion.3 = (f32[512,512]{1,0:T(8,128)}, f32[512,512]{1,0:T(8,128)}) fusion(bf16[512,512]{1,0:T(8,128)(2,1)S(1)} %add_convert_fusion, f32[512,512]{1,0:T(8,128)} %copy.25, f32[512]{0:T(512)S(1)} %copy-done.8, f32[512,512]{1,0:T(8,128)S(1)} %copy.23, f32[512]{0:T(512)S(1)} %broadcast_multiply_fusion, f32[512,512]{1,0:T(8,128)} %copy.22, ...), kind=kLoop, calls=%fused_computation.24 | loop fusion | flops 3932160 | bytes 5773312 | tf_op jit(solution)/shard_map/mul | solution.py:180
  42.9 0.0 copy-start.3
  42.9 5.4 %local_scan.1 = (f32[2,512]{1,0:T(2,128)}, f32[512,512]{1,0:T(8,128)}, f32[512,512]{1,0:T(8,128)}) custom-call(f32[512,512]{1,0:T(8,128)} %get-tuple-element.12.decay_ref, f32[512,512]{1,0:T(8,128)} %get-tuple-element.11.drive_ref), custom_call_target="tpu_custom_call" | custom-call | tf_op jit(solution)/shard_map/local_scan/pallas_call | solution.py:55
  48.3 9.3 %prefix.1 = f32[1,512]{1,0:T(1,128)} custom-call(f32[2,512]{1,0:T(2,128)} %get-tuple-element.10.ends_ref), custom_call_target="tpu_custom_call" | custom-call | tf_op jit(solution)/shard_map/prefix/pallas_call | solution.py:115
  57.6 0.0 copy-done.3
  57.6 2.0 %fusion.18 = bf16[512,512]{1,0:T(8,128)(2,1)S(1)} fusion(f32[512,512]{1,0:T(8,128)} %get-tuple-element.8, f32[512,512]{1,0:T(8,128)} %get-tuple-element.9, bf16[512,1024]{1,0:T(8,128)(2,1)S(1)} %copy-done.3, f32[512]{0:T(512)} %bitcast.37), kind=kLoop, calls=%fused_computation.23 | loop fusion | flops 3407872 | bytes 3147776 | tf_op jit(solution)/shard_map/convert_element_type | solution.py:183
  59.6 0.2 copy.26
  59.8 4.2 %all_to_all.19 = bf16[2,256,512]{1,2,0:T(8,128)(2,1)S(1)} all-to-all(bf16[2,256,512]{1,2,0:T(8,128)(2,1)S(1)} %copy.26), channel_id=1, replica_groups=mesh['sp'=16,'tp'=2] {'tp'}, dimensions={0} | all-to-all | bytes 1048576 | tf_op jit(solution)/shard_map/all_to_all | solution.py:184
  64.0 0.0 all-gather.5.cloned.1.call-done
  64.0 4.4 %convolution_convert_fusion = bf16[256,2048]{1,0:T(8,128)(2,1)} fusion(bf16[256,1024]{0,1:T(8,128)(2,1)S(1)} %bitcast.31, bf16[1024,2048]{1,0:T(8,128)(2,1)} %all-gather.5.cloned.1.call-done), kind=kOutput, calls=%fused_computation.6 | convolution fusion | flops 1074266112 | bytes 5767168 | tf_op jit(solution)/shard_map/dot_general | solution.py:186
  (6 shorter events, 0.1 us)
Async XLA Ops:
  6.5 29.0 %copy-start = (bf16[8,64,64]{2,1,0:T(8,128)(2,1)S(1)}, bf16[8,64,64]{2,1,0:T(8,128)(2,1)}, u32[]{:S(2)}) copy-start(bf16[8,64,64]{2,1,0:T(8,128)(2,1)} %param.17) | copy-start | bytes 196612
  6.5 3.2 %copy-start.1 = (bf16[256,2048]{1,0:T(8,128)(2,1)S(1)}, bf16[256,2048]{1,0:T(8,128)(2,1)}, u32[]{:S(2)}) copy-start(bf16[256,2048]{1,0:T(8,128)(2,1)} %param.12) | copy-start | bytes 3145732
  6.5 3.2 %copy-start.6 = (f32[2048]{0:T(1024)S(1)}, f32[2048]{0:T(1024)}, u32[]{:S(2)}) copy-start(f32[2048]{0:T(1024)} %param.13) | copy-start | bytes 24580
  6.5 18.1 %all-gather.3.cloned.1.call-start = ((), (), s32[]{:S(2)}) async-start(), calls=%async_computation.1 | async-start | bytes 3145728 | tf_op jit(solution)/shard_map/all_gather | solution.py:151
  11.1 0.8 %copy-start.7 = (f32[4,512]{1,0:T(4,128)S(1)}, f32[4,512]{1,0:T(4,128)}, u32[]{:S(2)}) copy-start(f32[4,512]{1,0:T(4,128)} %param.16) | copy-start | bytes 24580
  11.2 52.8 %all-gather.5.cloned.1.call-start = ((), (), s32[]{:S(2)}) async-start(), calls=%async_computation.2 | async-start | bytes 6291456 | tf_op jit(solution)/shard_map/all_gather | solution.py:185
  11.9 21.5 %copy-start.10 = (f32[512]{0:T(512)S(1)}, f32[512]{0:T(512)}, u32[]{:S(2)}) copy-start(f32[512]{0:T(512)} %param.21) | copy-start | bytes 6148
  11.9 21.5 %copy-start.5 = (f32[8,512]{1,0:T(8,128)S(1)}, f32[8,512]{1,0:T(8,128)}, u32[]{:S(2)}) copy-start(f32[8,512]{1,0:T(8,128)} %param.22) | copy-start | bytes 49156
  29.8 4.2 %copy-start.2 = (bf16[512,1024]{1,0:T(8,128)(2,1)}, bf16[512,1024]{1,0:T(8,128)(2,1)S(1)}, u32[]{:S(2)}) copy-start(bf16[512,1024]{1,0:T(8,128)(2,1)S(1)} %fusion.9) | copy-start | bytes 3145732
  29.8 5.0 %collective-permute-start = (bf16[3,512]{1,0:T(4,128)(2,1)S(1)}, bf16[3,512]{1,0:T(4,128)(2,1)S(1)}, u32[]{:S(2)}, u32[]{:S(2)}) collective-permute-start(bf16[3,512]{1,0:T(4,128)(2,1)S(1)} %slice.41), channel_id=1, source_target_pairs={{0,2},{2,4},{4,6},{6,8},{8,10},{10,12},{12,14},{14,16},{16,18},{18... | collective-permute-start | bytes 9224 | tf_op jit(solution)/shard_map/ppermute | solution.py:16
  35.5 1.7 %copy-start.4 = (bf16[8,64,64]{2,1,0:T(8,128)(2,1)S(1)}, bf16[8,64,64]{2,1,0:T(8,128)(2,1)}, u32[]{:S(2)}) copy-start(bf16[8,64,64]{2,1,0:T(8,128)(2,1)} %param.19) | copy-start | bytes 196612
  37.2 1.7 %copy-start.8 = (f32[512]{0:T(512)S(1)}, f32[512]{0:T(512)}, u32[]{:S(2)}) copy-start(f32[512]{0:T(512)} %param.20) | copy-start | bytes 6148
  37.2 1.7 %copy-start.9 = (f32[512]{0:T(512)S(1)}, f32[512]{0:T(512)}, u32[]{:S(2)}) copy-start(f32[512]{0:T(512)} %param.18) | copy-start | bytes 6148
  42.9 14.7 %copy-start.3 = (bf16[512,1024]{1,0:T(8,128)(2,1)S(1)}, bf16[512,1024]{1,0:T(8,128)(2,1)}, u32[]{:S(2)}) copy-start(bf16[512,1024]{1,0:T(8,128)(2,1)} %copy-done.2) | copy-start | bytes 3145732
Sparse Core Ops, SparseCore 0:
  11.3 13.2 all-gather.2
  26.1 14.8 all-gather.4
